TPU v7x, 32 devices: a whole 2x2x4 slice. The times are simulated.
32 devices in a mesh: fs: 16 (over z, y, x), tp: 2 (over core).
Axes of the slice: x: 2, y: 2, z: 4, core: 2. Of those that a mesh axis runs over, the one named last changes fastest.
Arguments:
- x_late: bfloat16 [4096, 2048], P('fs'), may hold values from -6 to 6
- x_early: bfloat16 [4096, 2048], P('fs'), may hold values from -6 to 6
- cotangent: bfloat16 [4096, 2048], P('fs'), may hold values from -6 to 6
- w_gate: bfloat16 [2048, 4096], P('fs', 'tp'), may hold values from -0.125 to 0.125
- w_up: bfloat16 [2048, 4096], P('fs', 'tp'), may hold values from -0.125 to 0.125
- w_down: bfloat16 [4096, 2048], P('tp', 'fs'), may hold values from -0.09375 to 0.09375
- conv_taps: float32 [3, 4096], replicated, may hold values from -3 to 3
- conv_bias: float32 [4096], replicated, may hold values from -3 to 3
- grad_down: float32 [4096, 2048], P('tp', 'fs'), may hold values from -60 to 60
Outputs:
- y_late: bfloat16 [4096, 2048], P('fs')
- dx_early: bfloat16 [4096, 2048], P('fs')
- grad_down_out: float32 [4096, 2048], P('tp', 'fs')
All inputs are finite; a program needn't handle non-finite values.
Results may differ from a plain program's by a relative error of at most 0.017.
Values may be sent and summed in bfloat16 or wider, within the bound.
A program may use at most 128 MiB of HBM per device.

v0:
```python
import jax
import jax.numpy as jnp
from jax import lax
from jax.sharding import PartitionSpec as P


def shift_later(field, steps):
    pad = jnp.zeros((steps, field.shape[1]), jnp.float32)
    return jnp.concatenate([pad, field[: field.shape[0] - steps]], axis=0)


def shift_earlier(field, steps):
    pad = jnp.zeros((steps, field.shape[1]), jnp.float32)
    return jnp.concatenate([field[steps:], pad], axis=0)


def contract_last(left, right):
    return lax.dot_general(
        left, right, (((1,), (1,)), ((), ())), preferred_element_type=jnp.float32
    )


def hidden_parts(inputs, gate_full, up_full, taps, bias):
    gate = (
        jnp.dot(inputs, gate_full, preferred_element_type=jnp.float32)
        .astype(jnp.bfloat16)
        .astype(jnp.float32)
    )
    up = jnp.dot(inputs, up_full, preferred_element_type=jnp.float32)
    conv = bias + taps[2] * gate + taps[1] * shift_later(gate, 1) + taps[0] * shift_later(gate, 2)
    act = jax.nn.silu(conv)
    hidden = (act * up).astype(jnp.bfloat16)
    return (conv, act, up, hidden)


def forward_pass(x_late, gate_full, up_full, down_full, taps, bias):
    conv, act, up, hidden = hidden_parts(x_late, gate_full, up_full, taps, bias)
    partial_value = jnp.dot(hidden, down_full, preferred_element_type=jnp.float32)
    return lax.psum(partial_value.astype(jnp.bfloat16), "tp")


def backward_pass(x_early, cotangent, gate_full, up_full, down_full, taps, bias, grad_down):
    conv, act, up, hidden = hidden_parts(x_early, gate_full, up_full, taps, bias)
    dhidden = contract_last(cotangent, down_full)
    summed = lax.psum_scatter(
        lax.dot_general(
            cotangent, hidden, (((0,), (0,)), ((), ())), preferred_element_type=jnp.float32
        ),
        "fs",
        scatter_dimension=0,
        tiled=True,
    )
    grad_down_out = grad_down + summed.T
    dup = (dhidden * act).astype(jnp.bfloat16)
    sig = jax.nn.sigmoid(conv)
    dconv = dhidden * up * sig * (1.0 + conv * (1.0 - sig))
    dgate = taps[2] * dconv + taps[1] * shift_earlier(dconv, 1) + taps[0] * shift_earlier(dconv, 2)
    dgate = dgate.astype(jnp.bfloat16)
    partial_value = contract_last(dup, up_full) + contract_last(dgate, gate_full)
    dx_early = lax.psum(partial_value.astype(jnp.bfloat16), "tp")
    return (dx_early, grad_down_out)


def shards(x_late, x_early, cotangent, w_gate, w_up, w_down, conv_taps, conv_bias, grad_down):
    width = w_gate.shape[1]
    offset = lax.axis_index("tp") * width
    taps = lax.dynamic_slice_in_dim(conv_taps, offset, width, 1)
    bias = lax.dynamic_slice_in_dim(conv_bias, offset, width, 0)
    gate_full, up_full = (
        lax.all_gather(w_gate, "fs", axis=0, tiled=True),
        lax.all_gather(w_up, "fs", axis=0, tiled=True),
    )
    down_full = lax.all_gather(w_down, "fs", axis=1, tiled=True)
    y_late = forward_pass(x_late, gate_full, up_full, down_full, taps, bias)
    dx_early, grad_down_out = backward_pass(
        x_early, cotangent, gate_full, up_full, down_full, taps, bias, grad_down
    )
    return (y_late, dx_early, grad_down_out)


def solution(mesh):
    placed = (
        P("fs", None),
        P("fs", None),
        P("fs", None),
        P("fs", "tp"),
        P("fs", "tp"),
        P("tp", "fs"),
        P(),
        P(),
        P("tp", "fs"),
    )
    return jax.shard_map(
        shards,
        mesh=mesh,
        in_specs=placed,
        out_specs=(P("fs", None), P("fs", None), P("tp", "fs")),
        check_vma=False,
    )
```

profile of v0, /device:TPU:0, one launch (start us, length us, event | category | flops | bytes accessed | tf_op | source)
XLA Modules:
  0.0 786.5 jit_solution(6254999555990808073)
XLA Ops:
  7.2 0.0 copy-start
  7.2 0.0 all-gather.4.cloned.1.call-start
  7.2 0.7 all-gather.4.cloned.1.call-update
  7.9 0.0 all-gather.6.cloned.1.call-start
  8.0 0.7 all-gather.6.cloned.1.call-update
  8.7 0.0 all-gather.8.cloned.1.call-start
  8.7 0.7 all-gather.8.cloned.1.call-update
  9.4 0.0 reduce-scatter.2.cloned.1.call-start
  9.4 0.7 dynamic_slice.6
  10.2 1.0 fusion.16
  11.1 0.0 copy-start.7
  11.1 114.7 %all-gather.4.cloned.1.call-done = bf16[2048,2048]{1,0:T(8,128)(2,1)} async-done(((bf16[128,2048]{1,0:T(8,128)(2,1)}), bf16[2048,2048]{1,0:T(8,128)(2,1)}) %all-gather.4.cloned.1.call-update) | async-done | bytes 8388624 | tf_op jit(solution)/shard_map/all_gather | solution.py:70
  125.8 7.4 fusion.2
  133.2 105.9 %all-gather.6.cloned.1.call-done = bf16[2048,2048]{1,0:T(8,128)(2,1)} async-done(((bf16[128,2048]{1,0:T(8,128)(2,1)}), bf16[2048,2048]{1,0:T(8,128)(2,1)}) %all-gather.6.cloned.1.call-update) | async-done | bytes 8388624 | tf_op jit(solution)/shard_map/all_gather | solution.py:71
  239.1 0.0 copy-done.7
  239.1 7.1 fusion.17
  246.2 135.7 %all-gather.8.cloned.1.call-done = bf16[2048,2048]{1,0:T(8,128)(2,1)} async-done(((bf16[2048,128]{1,0:T(8,128)(2,1)}), bf16[2048,2048]{1,0:T(8,128)(2,1)}) %all-gather.8.cloned.1.call-update) | async-done | bytes 8388624 | tf_op jit(solution)/shard_map/all_gather | solution.py:73
  381.8 0.0 copy-done
  381.8 0.0 copy-start.4
  381.8 10.6 %add_multiply_fusion = (f32[256,2048]{1,0:T(8,128)S(1)}, f32[256,2048]{1,0:T(8,128)S(1)}, f32[256,2048]{1,0:T(8,128)}) fusion(f32[256,2048]{1,0:T(8,128)} %fusion.17, f32[254,2048]{1,0:T(8,128)} %bitcast.38, f32[2048]{0:T(1024)S(1)} %bitcast.31, f32[255,2048]{1,0:T(8,128)} %bitcast.39, f32[2048]{0:T(1024)S(1)} %bitcast.28, f32[256,2048]{1,0:T(8,128)} %fusion.2, ...), kind=kOutput, calls=%fused_computation.12 | convolution fusion | flops 2155347968 | bytes 24125440 | tf_op jit(solution)/shard_map/dot_general | solution.py:18
  392.5 0.0 copy-start.2
  392.5 1.3 copy-done.2
  393.8 0.0 copy-done.4
  393.8 8.2 %convolution_bitcast_fusion = f32[2048,2048]{0,1:T(8,128)} fusion(bf16[256,2048]{1,0:T(8,128)(2,1)S(1)} %copy-done, f32[256,2048]{1,0:T(8,128)S(1)} %copy-done.4, f32[256,2048]{1,0:T(8,128)S(1)} %get-tuple-element.6), kind=kOutput, calls=%fused_computation | convolution fusion | flops 2150629376 | bytes 22020096 | tf_op jit(solution)/shard_map/dot_general | solution.py:46
  402.0 0.0 reduce-scatter.2.cloned.1.call-update
  402.0 0.2 all-reduce.9.cloned.1.call-start
  402.2 0.0 copy-start.8
  402.2 0.2 slice.47
  402.4 0.0 slice-start
  402.4 0.2 slice.46
  402.6 0.8 copy-done.8
  403.5 0.0 copy-start.3
  403.5 0.0 copy-start.9
  403.5 0.0 slice-start.1
  403.5 8.4 %fusion.3 = f32[256,2048]{1,0:T(8,128)} fusion(bf16[256,2048]{1,0:T(8,128)(2,1)S(1)} %copy-done.8, bf16[2048,2048]{1,0:T(8,128)(2,1)} %all-gather.4.cloned.1.call-done), kind=kOutput, calls=%fused_computation.9 | convolution fusion | flops 2148532224 | bytes 11534336 | tf_op jit(solution)/shard_map/dot_general | solution.py:25
  411.8 0.0 copy-done.3
  411.8 0.0 copy-done.9
  411.8 7.2 fusion.5
  419.0 0.0 slice-done
  419.0 0.0 slice-done.1
  419.0 5.1 fusion
  424.1 13.8 %convolution_convert_fusion.1 = bf16[256,2048]{1,0:T(8,128)(2,1)} fusion(bf16[2048,2048]{1,0:T(8,128)(2,1)} %all-gather.8.cloned.1.call-done, bf16[256,2048]{1,0:T(8,128)(2,1)S(1)} %copy-done.8, bf16[2048,2048]{1,0:T(8,128)(2,1)} %all-gather.6.cloned.1.call-done, f32[254,2048]{1,0:T(8,128)} %bitcast.36, f32[255,2048]{1,0:T(8,128)} %bitcast.37, ...), kind=kOutput, calls=%fused_computation.7 | convolution fusion | flops 4301783040 | bytes 25174016 | tf_op jit(solution)/shard_map/dot_general | solution.py:38
  437.9 0.0 copy-start.5
  437.9 0.0 all-reduce.9.cloned.1.call-update
  437.9 308.8 %reduce-scatter.2.cloned.1.call-done = f32[128,2048]{0,1:T(8,128)} async-done(((f32[2048,2048]{0,1:T(8,128)}), f32[128,2048]{0,1:T(8,128)}) %reduce-scatter.2.cloned.1.call-update) | async-done | bytes 1048592 | tf_op jit(solution)/shard_map/reduce_scatter | solution.py:45
  746.8 0.0 copy-done.5
  746.8 2.3 bitcast_add_fusion
  749.1 27.5 %all-reduce.9.cloned.1.call-done = (bf16[256,2048]{1,0:T(8,128)(2,1)}, bf16[256,2048]{1,0:T(8,128)(2,1)}) async-done(((bf16[256,2048]{1,0:T(8,128)(2,1)}, bf16[256,2048]{1,0:T(8,128)(2,1)}), (bf16[256,2048]{1,0:T(8,128)(2,1)}, bf16[256,2048]{1,0:T(8,128)(2,1)})) %all-reduce.9.cloned.1.call-update) | async-done | bytes 2097168 | tf_op jit(solution)/shard_map/psum | solution.py:39
  776.6 0.0 copy-start.6
  776.6 0.0 copy-start.1
  776.6 2.5 copy.14
  779.0 0.0 copy-done.6
  779.0 1.0 copy.15
  780.0 0.0 copy-done.1
  (1 shorter events, 0.0 us)
Async XLA Ops:
  7.2 374.7 %copy-start = (bf16[256,2048]{1,0:T(8,128)(2,1)S(1)}, bf16[256,2048]{1,0:T(8,128)(2,1)}, u32[]{:S(2)}) copy-start(bf16[256,2048]{1,0:T(8,128)(2,1)} %param.11) | copy-start | bytes 3145732
  7.2 118.6 %all-gather.4.cloned.1.call-start = ((), (), s32[]{:S(2)}) async-start(), calls=%async_computation.1 | async-start | bytes 8912896 | tf_op jit(solution)/shard_map/all_gather | solution.py:70
  7.9 231.2 %all-gather.6.cloned.1.call-start = ((), (), s32[]{:S(2)}) async-start(), calls=%async_computation.2 | async-start | bytes 8912896 | tf_op jit(solution)/shard_map/all_gather | solution.py:71
  8.7 373.2 %all-gather.8.cloned.1.call-start = ((), (), s32[]{:S(2)}) async-start(), calls=%async_computation.3 | async-start | bytes 8912896 | tf_op jit(solution)/shard_map/all_gather | solution.py:73
  9.4 737.4 %reduce-scatter.2.cloned.1.call-start = ((), (), s32[]{:S(2)}) async-start(), calls=%async_computation.4 | async-start | bytes 17825792 | tf_op jit(solution)/shard_map/reduce_scatter | solution.py:45
  11.1 228.0 %copy-start.7 = (bf16[256,2048]{1,0:T(8,128)(2,1)S(1)}, bf16[256,2048]{1,0:T(8,128)(2,1)}, u32[]{:S(2)}) copy-start(bf16[256,2048]{1,0:T(8,128)(2,1)} %param.10) | copy-start | bytes 3145732
  381.8 11.9 %copy-start.4 = (f32[256,2048]{1,0:T(8,128)S(1)}, f32[256,2048]{1,0:T(8,128)}, u32[]{:S(2)}) copy-start(f32[256,2048]{1,0:T(8,128)} %fusion.17) | copy-start | bytes 6291460
  392.5 1.3 copy-start.2
  402.0 374.6 %all-reduce.9.cloned.1.call-start = ((), (), s32[]{:S(2)}) async-start(), calls=%async_computation.5 | async-start | bytes 4194304 | tf_op jit(solution)/shard_map/psum | solution.py:39
  402.2 1.2 copy-start.8
  402.4 16.6 %slice-start = ((s8[8388608]{0:T(1024)(128)(4,1)}), s8[4194304]{0:T(1024)(128)(4,1)S(1)}, s32[]{:S(2)}) async-start(s8[8388608]{0:T(1024)(128)(4,1)} %bitcast.34), calls=%async_computation.6 | async-start | bytes 8388608
  403.5 8.4 %copy-start.3 = (f32[256,2048]{1,0:T(8,128)S(1)}, f32[256,2048]{1,0:T(8,128)}, u32[]{:S(2)}) copy-start(f32[256,2048]{1,0:T(8,128)} %copy-done.2) | copy-start | bytes 6291460
  403.5 8.4 %copy-start.9 = (f32[256,2048]{1,0:T(8,128)S(1)}, f32[256,2048]{1,0:T(8,128)}, u32[]{:S(2)}) copy-start(f32[256,2048]{1,0:T(8,128)} %get-tuple-element.10) | copy-start | bytes 6291460
  403.5 15.5 %slice-start.1 = ((s8[8388608]{0:T(1024)(128)(4,1)}), s8[4194304]{0:T(1024)(128)(4,1)S(1)}, s32[]{:S(2)}) async-start(s8[8388608]{0:T(1024)(128)(4,1)} %bitcast.34), calls=%async_computation.7 | async-start | bytes 8388608
  437.9 308.8 %copy-start.5 = (f32[2048,128]{1,0:T(8,128)S(1)}, f32[2048,128]{1,0:T(8,128)}, u32[]{:S(2)}) copy-start(f32[2048,128]{1,0:T(8,128)} %param.17) | copy-start | bytes 3145732
  776.6 2.5 copy-start.6
  776.6 3.4 copy-start.1
Sparse Core Ops, SparseCore 0:
  10.8 115.0 all-gather.3
  128.6 110.4 all-gather.5
  241.8 139.9 all-gather.7
  402.1 344.5 reduce-scatter.1
  749.6 26.9 all-reduce.8
where the time goes:
time: 787 us
  waiting for transfers between devices  695 us (88%)
  matrix products  67.7 us (9%)
  between operations  13.9 us (2%)
    reduce_scatter x1, waiting for transfers between devices, backward_pass(): lax.psum_scatter(lax.dot_general(cotangent, hidden, (((0,), (0,)), ((), (...  309 us
    all_gather x1, waiting for transfers between devices, shards(): down_full = lax.all_gather(w_down, 'fs', axis=1, tiled=True)  136 us
    all_gather x1, waiting for transfers between devices, shards(): lax.all_gather(w_gate, 'fs', axis=0, tiled=True)  115 us
    all_gather x1, waiting for transfers between devices, shards(): lax.all_gather(w_up, 'fs', axis=0, tiled=True)  106 us
    psum x1, waiting for transfers between devices, forward_pass(): return lax.psum(partial_value.astype(jnp.bfloat16), 'tp')  27.5 us
    dot_general x3, matrix products, contract_last(): lax.dot_general(left, right, (((1,), (1,)), ((), ())), preferred_element_...  22.9 us
    dot_general x2, matrix products, hidden_parts(): jnp.dot(inputs, gate_full, preferred_element_type=jnp.float32)  15.7 us
  transfers between devices with their start and end apart: 5, of which 5 were waited for; matrix products, arithmetic and copies ran while one was open for 7% of the time, Pallas kernels for 0%

commit v1 on v0

--- a/solution.py
+++ b/solution.py
@@ -70,7 +70,7 @@
         lax.all_gather(w_gate, "fs", axis=0, tiled=True),
         lax.all_gather(w_up, "fs", axis=0, tiled=True),
     )
-    down_full = lax.all_gather(w_down, "fs", axis=1, tiled=True)
+    down_full = jnp.concatenate(lax.all_gather(w_down, "fs"), 1)
     y_late = forward_pass(x_late, gate_full, up_full, down_full, taps, bias)
     dx_early, grad_down_out = backward_pass(
         x_early, cotangent, gate_full, up_full, down_full, taps, bias, grad_down

time: 787 us -> 758 us (0.963)
  waiting for transfers between devices: 695 us -> 663 us
  local copies, waits for them, and re-layouts: 7.64 us -> 20.6 us
  matrix products: 67.7 us -> 57.5 us
    all_gather x1, waiting for transfers between devices: 136 us -> 115 us  [shards(): down_full = jnp.concatenate(lax.all_gather(w_down, 'fs'), 1)]
    all_gather x1, waiting for transfers between devices: 115 us -> 101 us  [shards(): lax.all_gather(w_gate, 'fs', axis=0, tiled=True)]
    reshape x0 -> x1, local copies, waits for them, and re-layouts: none -> 12.5 us  [shards(): down_full = jnp.concatenate(lax.all_gather(w_down, 'fs'), 1)]
    dot_general x3, matrix products: 22.9 us -> 14.2 us  [contract_last(): lax.dot_general(left, right, (((1,), (1,)), ((), ())), preferred_element_...]
where the time goes in v1:
time: 758 us
  waiting for transfers between devices  663 us (87%)
  matrix products  57.5 us (8%)
  local copies, waits for them, and re-layouts  20.6 us (3%)
  between operations  13.9 us (2%)
    reduce_scatter x1, waiting for transfers between devices, backward_pass(): lax.psum_scatter(lax.dot_general(cotangent, hidden, (((0,), (0,)), ((), (...  312 us
    all_gather x1, waiting for transfers between devices, shards(): down_full = jnp.concatenate(lax.all_gather(w_down, 'fs'), 1)  115 us
    all_gather x1, waiting for transfers between devices, shards(): lax.all_gather(w_up, 'fs', axis=0, tiled=True)  106 us
    all_gather x1, waiting for transfers between devices, shards(): lax.all_gather(w_gate, 'fs', axis=0, tiled=True)  101 us
    psum x1, waiting for transfers between devices, forward_pass(): return lax.psum(partial_value.astype(jnp.bfloat16), 'tp')  27.6 us
    dot_general x2, matrix products, hidden_parts(): jnp.dot(inputs, gate_full, preferred_element_type=jnp.float32)  15.4 us
  transfers between devices with their start and end apart: 5, of which 5 were waited for; matrix products, arithmetic and copies ran while one was open for 7% of the time, Pallas kernels for 0%

profile of v1, /device:TPU:0, one launch (start us, length us, event | category | flops | bytes accessed | tf_op | source)
XLA Modules:
  0.0 757.7 jit_solution(6112805274584227047)
XLA Ops:
  7.2 0.0 copy-start
  7.2 0.0 all-gather.9.cloned.1.call-start
  7.2 0.7 all-gather.9.cloned.1.call-update
  7.9 0.0 all-gather.5.cloned.1.call-start
  8.0 0.7 all-gather.5.cloned.1.call-update
  8.7 0.0 all-gather.7.cloned.1.call-start
  8.7 0.7 all-gather.7.cloned.1.call-update
  9.4 0.0 reduce-scatter.2.cloned.1.call-start
  9.4 0.7 dynamic_slice.6
  10.2 1.0 fusion.16
  11.1 114.7 %all-gather.9.cloned.1.call-done = bf16[32768,128]{1,0:T(8,128)(2,1)} async-done(((bf16[2048,128]{1,0:T(8,128)(2,1)}), bf16[32768,128]{1,0:T(8,128)(2,1)}) %all-gather.9.cloned.1.call-update) | async-done | bytes 8388624 | tf_op jit(solution)/shard_map/all_gather | solution.py:73
  125.8 0.0 copy-start.7
  125.8 12.5 %copy.12 = bf16[2048,16,128]{0,2,1:T(8,128)(2,1)} copy(bf16[2048,16,128]{2,0,1:T(8,128)(2,1)} %bitcast.29) | data formatting | bytes 16777216 | tf_op jit(solution)/shard_map/reshape | solution.py:73
  138.3 100.8 %all-gather.5.cloned.1.call-done = bf16[2048,2048]{1,0:T(8,128)(2,1)} async-done(((bf16[128,2048]{1,0:T(8,128)(2,1)}), bf16[2048,2048]{1,0:T(8,128)(2,1)}) %all-gather.5.cloned.1.call-update) | async-done | bytes 8388624 | tf_op jit(solution)/shard_map/all_gather | solution.py:70
  239.1 0.0 copy-done.7
  239.1 7.1 fusion.2
  246.1 106.2 %all-gather.7.cloned.1.call-done = bf16[2048,2048]{1,0:T(8,128)(2,1)} async-done(((bf16[128,2048]{1,0:T(8,128)(2,1)}), bf16[2048,2048]{1,0:T(8,128)(2,1)}) %all-gather.7.cloned.1.call-update) | async-done | bytes 8388624 | tf_op jit(solution)/shard_map/all_gather | solution.py:71
  352.4 0.0 copy-start.2
  352.4 0.0 copy-start.9
  352.4 5.9 fusion.17
  358.2 0.0 copy-done
  358.2 0.0 copy-done.2
  358.3 0.5 copy-done.9
  358.7 4.9 add_multiply_fusion
  363.6 0.0 copy-start.3
  363.6 1.3 copy-done.3
  364.9 8.2 %convolution_bitcast_fusion = f32[2048,2048]{0,1:T(8,128)} fusion(bf16[256,2048]{1,0:T(8,128)(2,1)S(1)} %copy-done, f32[256,2048]{1,0:T(8,128)S(1)} %fusion.17, f32[256,2048]{1,0:T(8,128)S(1)} %get-tuple-element.6), kind=kOutput, calls=%fused_computation | convolution fusion | flops 2150629376 | bytes 22020096 | tf_op jit(solution)/shard_map/dot_general | solution.py:46
  373.1 0.0 reduce-scatter.2.cloned.1.call-update
  373.2 0.2 all-reduce.9.cloned.1.call-start
  373.4 0.0 copy-start.8
  373.4 0.2 slice.47
  373.6 0.0 slice-start
  373.6 0.2 slice.46
  373.8 0.8 copy-done.8
  374.6 0.0 copy-start.4
  374.6 0.0 copy-start.10
  374.6 0.0 slice-start.1
  374.6 8.4 %fusion.3 = f32[256,2048]{1,0:T(8,128)} fusion(bf16[256,2048]{1,0:T(8,128)(2,1)S(1)} %copy-done.8, bf16[2048,2048]{1,0:T(8,128)(2,1)} %all-gather.5.cloned.1.call-done), kind=kOutput, calls=%fused_computation.9 | convolution fusion | flops 2148532224 | bytes 11534336 | tf_op jit(solution)/shard_map/dot_general | solution.py:25
  383.0 0.0 copy-done.4
  383.0 0.0 copy-done.10
  383.0 5.8 fusion.5
  388.8 0.0 slice-done
  388.8 0.0 slice-done.1
  388.9 3.5 fusion
  392.4 13.8 %convolution_convert_fusion.1 = bf16[256,2048]{1,0:T(8,128)(2,1)} fusion(bf16[2048,2048]{0,1:T(8,128)(2,1)} %bitcast.30, bf16[256,2048]{1,0:T(8,128)(2,1)S(1)} %copy-done.8, bf16[2048,2048]{1,0:T(8,128)(2,1)} %all-gather.7.cloned.1.call-done, f32[254,2048]{1,0:T(8,128)} %bitcast.43, f32[255,2048]{1,0:T(8,128)} %bitcast.44, f32[256,2048]{1,0:T(8,128)} %fusion.3, ...), kind=kOutput, calls=%fused_computation.7 | convolution fusion | flops 4301783040 | bytes 25174016 | tf_op jit(solution)/shard_map/dot_general | solution.py:38
  406.2 0.0 copy-start.5
  406.2 0.0 all-reduce.9.cloned.1.call-update
  406.2 311.7 %reduce-scatter.2.cloned.1.call-done = f32[128,2048]{0,1:T(8,128)} async-done(((f32[2048,2048]{0,1:T(8,128)}), f32[128,2048]{0,1:T(8,128)}) %reduce-scatter.2.cloned.1.call-update) | async-done | bytes 1048592 | tf_op jit(solution)/shard_map/reduce_scatter | solution.py:45
  717.9 0.0 copy-done.5
  717.9 2.3 bitcast_add_fusion
  720.2 27.6 %all-reduce.9.cloned.1.call-done = (bf16[256,2048]{1,0:T(8,128)(2,1)}, bf16[256,2048]{1,0:T(8,128)(2,1)}) async-done(((bf16[256,2048]{1,0:T(8,128)(2,1)}, bf16[256,2048]{1,0:T(8,128)(2,1)}), (bf16[256,2048]{1,0:T(8,128)(2,1)}, bf16[256,2048]{1,0:T(8,128)(2,1)})) %all-reduce.9.cloned.1.call-update) | async-done | bytes 2097168 | tf_op jit(solution)/shard_map/psum | solution.py:39
  747.8 0.0 copy-start.6
  747.8 0.0 copy-start.1
  747.8 2.5 copy.15
  750.2 0.0 copy-done.6
  750.2 1.0 copy.16
  751.2 0.0 copy-done.1
  (1 shorter events, 0.0 us)
Async XLA Ops:
  7.2 351.1 %copy-start = (bf16[256,2048]{1,0:T(8,128)(2,1)S(1)}, bf16[256,2048]{1,0:T(8,128)(2,1)}, u32[]{:S(2)}) copy-start(bf16[256,2048]{1,0:T(8,128)(2,1)} %param.11) | copy-start | bytes 3145732
  7.2 118.6 %all-gather.9.cloned.1.call-start = ((), (), s32[]{:S(2)}) async-start(), calls=%async_computation.4 | async-start | bytes 8912896 | tf_op jit(solution)/shard_map/all_gather | solution.py:73
  7.9 231.2 %all-gather.5.cloned.1.call-start = ((), (), s32[]{:S(2)}) async-start(), calls=%async_computation.1 | async-start | bytes 8912896 | tf_op jit(solution)/shard_map/all_gather | solution.py:70
  8.7 343.7 %all-gather.7.cloned.1.call-start = ((), (), s32[]{:S(2)}) async-start(), calls=%async_computation.2 | async-start | bytes 8912896 | tf_op jit(solution)/shard_map/all_gather | solution.py:71
  9.4 708.5 %reduce-scatter.2.cloned.1.call-start = ((), (), s32[]{:S(2)}) async-start(), calls=%async_computation.3 | async-start | bytes 17825792 | tf_op jit(solution)/shard_map/reduce_scatter | solution.py:45
  125.8 113.3 %copy-start.7 = (bf16[256,2048]{1,0:T(8,128)(2,1)S(1)}, bf16[256,2048]{1,0:T(8,128)(2,1)}, u32[]{:S(2)}) copy-start(bf16[256,2048]{1,0:T(8,128)(2,1)} %param.10) | copy-start | bytes 3145732
  352.4 5.9 copy-start.2
  352.4 6.4 copy-start.9
  363.6 1.3 copy-start.3
  373.2 374.6 %all-reduce.9.cloned.1.call-start = ((), (), s32[]{:S(2)}) async-start(), calls=%async_computation.5 | async-start | bytes 4194304 | tf_op jit(solution)/shard_map/psum | solution.py:39
  373.4 1.2 copy-start.8
  373.6 15.2 %slice-start = ((s8[8388608]{0:T(1024)(128)(4,1)}), s8[4194304]{0:T(1024)(128)(4,1)S(1)}, s32[]{:S(2)}) async-start(s8[8388608]{0:T(1024)(128)(4,1)} %bitcast.41), calls=%async_computation.6 | async-start | bytes 8388608
  374.6 8.4 %copy-start.4 = (f32[256,2048]{1,0:T(8,128)S(1)}, f32[256,2048]{1,0:T(8,128)}, u32[]{:S(2)}) copy-start(f32[256,2048]{1,0:T(8,128)} %copy-done.3) | copy-start | bytes 6291460
  374.6 8.4 %copy-start.10 = (f32[256,2048]{1,0:T(8,128)S(1)}, f32[256,2048]{1,0:T(8,128)}, u32[]{:S(2)}) copy-start(f32[256,2048]{1,0:T(8,128)} %get-tuple-element.10) | copy-start | bytes 6291460
  374.6 14.2 %slice-start.1 = ((s8[8388608]{0:T(1024)(128)(4,1)}), s8[4194304]{0:T(1024)(128)(4,1)S(1)}, s32[]{:S(2)}) async-start(s8[8388608]{0:T(1024)(128)(4,1)} %bitcast.41), calls=%async_computation.7 | async-start | bytes 8388608
  406.2 311.7 %copy-start.5 = (f32[2048,128]{1,0:T(8,128)S(1)}, f32[2048,128]{1,0:T(8,128)}, u32[]{:S(2)}) copy-start(f32[2048,128]{1,0:T(8,128)} %param.17) | copy-start | bytes 3145732
  747.8 2.5 copy-start.6
  747.8 3.4 copy-start.1
Sparse Core Ops, SparseCore 0:
  10.8 115.0 all-gather.8
  128.6 110.4 all-gather.4
  241.9 110.4 all-gather.6
  373.3 344.5 reduce-scatter.1
  720.7 27.0 all-reduce.8
